TPU v7x, 512 devices: a whole 4x4x16 slice. The times are simulated.
512 devices in a mesh: sp: 64 (over z, y), tp: 8 (over x, core).
Axes of the slice: x: 4, y: 4, z: 16, core: 2. Of those that a mesh axis runs over, the one named last changes fastest.
Arguments:
- stream: bfloat16 [16384, 2048], P(('sp', 'tp')), may hold values from -6 to 6
- queries: bfloat16 [16384, 1024], P('sp', 'tp'), may hold values from -6 to 6
- keys_in: bfloat16 [16384, 1024], P('sp', 'tp'), may hold values from -6 to 6
- values_in: bfloat16 [16384, 1024], P('sp', 'tp'), may hold values from -6 to 6
- gate_in: bfloat16 [16384, 1024], P('sp', 'tp'), may hold values from -6 to 6
- log_decay: float32 [16384, 8], P('sp', 'tp'), may hold values from -0.8 to 0
- head_gain: bfloat16 [1024], P('tp'), may hold values from 0.099609375 to 1.8984375
- out_weight: bfloat16 [1024, 2048], P('tp'), may hold values from -0.1875 to 0.1875
- norm_gain: bfloat16 [2048], replicated, may hold values from 0.099609375 to 1.8984375
- gate_weight: bfloat16 [2048, 5632], P('sp', 'tp'), may hold values from -0.125 to 0.125
- up_weight: bfloat16 [2048, 5632], P('sp', 'tp'), may hold values from -0.125 to 0.125
- down_weight: bfloat16 [5632, 2048], P('tp', 'sp'), may hold values from -0.078125 to 0.078125
Outputs:
- result: bfloat16 [16384, 2048], P(('sp', 'tp'))
All inputs are finite; a program needn't handle non-finite values.
Results may differ from a plain program's by a relative error of at most 0.02.
Values may be sent and summed in bfloat16 or wider, within the bound.
No kernel may reach another device: no remote copies, remote signals or barrier semaphores. Data moves between devices by JAX's collectives and lax.ppermute only.
A program may use at most 64 MiB of HBM per device.

v0:
```python
import jax
import jax.numpy as jnp
from jax import lax
from jax.experimental import pallas as pl
from jax.experimental.pallas import tpu as pltpu
from jax.sharding import Mesh
from jax.sharding import PartitionSpec as P


Z, Y = ("zh", "zl"), ("y1", "y0")
NEAR = ("zl",) + Y
SP = Z + Y
TP = ("x", "c")
GROUP = ("y0", "x")
SIZES = {"zh": 4, "zl": 4, "y1": 2, "y0": 2, "x": 4, "c": 2}
EPS = 1e-6
NEIGHBOURS = 16
F32, BF16 = jnp.float32, jnp.bfloat16


def vmem(count):
    return [pl.BlockSpec(memory_space=pltpu.VMEM)] * count


def kernel_cost(flops, moved, exps=0):
    return pl.CostEstimate(flops=flops, bytes_accessed=moved, transcendentals=exps)


def dot(a, b):
    return jnp.dot(a, b, preferred_element_type=F32)


def dot_nt(a, b):
    return lax.dot_general(a, b, (((1,), (1,)), ((), ())), preferred_element_type=F32)


def dot_tn(a, b):
    return lax.dot_general(a, b, (((0,), (0,)), ((), ())), preferred_element_type=F32)


def packed_state(state, total):
    width = state.shape[1]
    total = jnp.broadcast_to(total, (8, width))
    high = total.astype(BF16).astype(F32)
    mid = (total - high).astype(BF16).astype(F32)
    line = lax.broadcasted_iota(jnp.int32, total.shape, 0)
    terms = jnp.where(line == 0, high, jnp.where(line == 1, mid, total - high - mid))
    return jnp.concatenate([state, terms], axis=0).astype(BF16)


def unpacked_state(packed):
    part = packed.shape[0] - 8
    wide = packed.astype(F32)
    total = wide[part : part + 1] + wide[part + 1 : part + 2] + wide[part + 2 : part + 3]
    return wide[:part], total


def retention_kernel(q_ref, k_ref, v_ref, decay_ref, within_ref, carry_q_ref, state_ref):
    rows, head_dim = q_ref.shape
    scale = head_dim**-0.5
    at = lax.broadcasted_iota(jnp.int32, (rows, rows), 0)
    to = lax.broadcasted_iota(jnp.int32, (rows, rows), 1)
    causal = at >= to
    running = jnp.sum(jnp.where(causal, decay_ref[...], 0.0), axis=1, keepdims=True)
    across = jnp.sum(jnp.where(at == to, running, 0.0), axis=0, keepdims=True)
    total = running[rows - 1 : rows, :]
    q, k, v = q_ref[...], k_ref[...], v_ref[...]
    table = jnp.where(causal, jnp.exp(jnp.minimum(running - across, 0.0)), 0.0)
    scores = dot_nt(q, k) * scale
    within_ref[...] = dot((scores * table).astype(BF16), v)
    carry_q_ref[...] = (q.astype(F32) * jnp.exp(running)).astype(BF16)
    key_wide = (k.astype(F32) * scale * jnp.exp(total - running)).astype(BF16)
    state = dot_tn(key_wide, v)
    slices = state_ref.shape[0]
    part = head_dim // slices
    for n in range(slices):
        state_ref[n] = packed_state(state[n * part : (n + 1) * part], total)


def retention(q, k, v, decay):
    rows, head_dim = q.shape
    part = head_dim // NEIGHBOURS
    return pl.pallas_call(
        retention_kernel,
        out_shape=(
            jax.ShapeDtypeStruct((rows, head_dim), F32),
            jax.ShapeDtypeStruct((rows, head_dim), BF16),
            jax.ShapeDtypeStruct((NEIGHBOURS, part + 8, head_dim), BF16),
        ),
        in_specs=vmem(4),
        out_specs=vmem(3),
        cost_estimate=kernel_cost(6 * rows * rows * head_dim, 2**20, rows * rows),
        name="retention",
    )(q, k, v, decay)


def joined_kernel(states_ref, out_ref):
    state, total = unpacked_state(states_ref[0])
    for n in range(1, states_ref.shape[0]):
        own, decay = unpacked_state(states_ref[n])
        state = jnp.exp(decay) * state + own
        total = total + decay
    packed = packed_state(state, total)
    for n in range(out_ref.shape[0]):
        out_ref[n] = packed


def joined_state(states):
    _, lines, width = states.shape
    return pl.pallas_call(
        joined_kernel,
        out_shape=jax.ShapeDtypeStruct((SIZES["zh"], lines, width), BF16),
        in_specs=vmem(1),
        out_specs=pl.BlockSpec(memory_space=pltpu.VMEM),
        cost_estimate=kernel_cost(2**18, 2**18, 2**10),
        compiler_params=pltpu.CompilerParams(vmem_limit_bytes=2 * 2**20),
        name="joined_state",
    )(states)


def incoming_kernel(here_ref, joined_ref, states_ref, out_ref):
    here = here_ref[0]
    carried = jnp.zeros(out_ref.shape[1:], F32)
    for n in range(joined_ref.shape[0]):
        own, decay = unpacked_state(joined_ref[n])
        carried = jnp.where(n < here, jnp.exp(decay) * carried + own, carried)
    for n in range(out_ref.shape[0]):
        out_ref[n] = carried.astype(BF16)
        own, decay = unpacked_state(states_ref[n])
        carried = jnp.exp(decay) * carried + own


def incoming_state(here, joined, states):
    count, lines, width = states.shape
    return pl.pallas_call(
        incoming_kernel,
        out_shape=jax.ShapeDtypeStruct((count, lines - 8, width), BF16),
        in_specs=[pl.BlockSpec(memory_space=pltpu.SMEM)] + vmem(2),
        out_specs=pl.BlockSpec(memory_space=pltpu.VMEM),
        cost_estimate=kernel_cost(2**19, 2**19, 2**12),
        compiler_params=pltpu.CompilerParams(vmem_limit_bytes=2 * 2**20),
        name="incoming_state",
    )(here, joined, states)


def mix_kernel(within_ref, carry_q_ref, state_ref, gate_ref, gain_ref, out_ref):
    retained = within_ref[...] + dot(carry_q_ref[...], state_ref[...])
    center = jnp.mean(retained, axis=-1, keepdims=True)
    off = retained - center
    spread = jnp.mean(off * off, axis=-1, keepdims=True)
    normed = off * lax.rsqrt(spread + EPS) * gain_ref[...].astype(F32)
    gate = gate_ref[...].astype(F32)
    mixed = (gate * jax.nn.sigmoid(gate) * normed).astype(BF16)
    places, cores, blocks, lines, _ = out_ref.shape
    for core in range(cores):
        for n in range(blocks):
            first = (n * cores + core) * lines
            piece = mixed[first : first + lines]
            for place in range(places):
                out_ref[place, core, n] = piece


def mix(within, carry_q, state, gate, gain):
    rows, width = within.shape
    return pl.pallas_call(
        mix_kernel,
        out_shape=jax.ShapeDtypeStruct((8, 2, 4, rows // 8, width), BF16),
        in_specs=vmem(5),
        out_specs=pl.BlockSpec(memory_space=pltpu.VMEM),
        cost_estimate=kernel_cost(2 * rows * width * width, 2**20, rows * width),
        name="mix",
    )(within, carry_q, state, gate, gain)


def rows_kernel(
    here_ref, mixed_ref, near_w_ref, far_w_ref, near_s_ref, far_s_ref, gain_ref, normed_ref, own_ref, residual, normed, sems
):
    halves, _, blocks, lines, head_dim = mixed_ref.shape
    count, width = normed_ref.shape
    x, c, y0 = here_ref[0], here_ref[1], here_ref[2]

    def heads_of(core):
        return jnp.concatenate(
            [
                jnp.concatenate(
                    [mixed_ref[n, ((x + 4 - r) % 4) * 2 + core].reshape(count // halves, head_dim) for r in range(4)],
                    axis=1,
                )
                for n in range(halves)
            ],
            axis=0,
        )

    near, far = heads_of(c), heads_of(1 - c)
    step = width // 4
    squares = jnp.zeros((count, 1), F32)
    for n in range(4):
        span = slice(n * step, (n + 1) * step)
        rows = []
        for half in range(halves):
            for block in range(blocks):
                at = (x + 4 - block) % 4
                rows.append(jnp.where(y0 == half, near_s_ref[at, :, span], far_s_ref[at, :, span]))
        part = (
            jnp.concatenate(rows, axis=0).astype(F32)
            + dot(near, near_w_ref[:, span])
            + dot(far, far_w_ref[:, span])
        )
        residual[:, span] = part
        squares += jnp.sum(part * part, axis=-1, keepdims=True)
    factor = lax.rsqrt(squares / width + EPS)
    copies = []
    for n in range(4):
        span = slice(n * step, (n + 1) * step)
        normed[:, span] = (residual[:, span] * factor * gain_ref[:, span].astype(F32)).astype(BF16)
        copies.append(pltpu.make_async_copy(normed.at[:, span], normed_ref.at[:, span], sems.at[n]))
        copies[n].start()
    first = pl.multiple_of((y0 * blocks + x) * lines, lines)
    own_ref[...] = residual[pl.ds(first, lines), :]
    for copy in copies:
        copy.wait()


def group_rows(here, mixed, near_w, far_w, near_s, far_s, gain):
    lines, width = near_s.shape[1:]
    count = 8 * lines
    return pl.pallas_call(
        rows_kernel,
        out_shape=(
            jax.ShapeDtypeStruct((count, width), BF16),
            jax.ShapeDtypeStruct((lines, width), F32),
        ),
        in_specs=[pl.BlockSpec(memory_space=pltpu.SMEM)] + vmem(6),
        out_specs=[pl.BlockSpec(memory_space=pltpu.HBM)] + vmem(1),
        scratch_shapes=[
            pltpu.VMEM((count, width), F32),
            pltpu.VMEM((count, width), BF16),
            pltpu.SemaphoreType.DMA((4,)),
        ],
        cost_estimate=kernel_cost(2 * count * width * 1024, 2**23),
        compiler_params=pltpu.CompilerParams(vmem_limit_bytes=20 * 2**20),
        name="group_rows",
    )(here, mixed, near_w, far_w, near_s, far_s, gain)


CHUNKS = (2, 1, 1)
AHEAD = 2


def ffn_kernel(rows_ref, weight_ref, out_ref, rows, held, rows_sem, sems):
    z, _, _, kinds, lines, hidden_width = weight_ref.shape

    def copies(kind, n):
        each = z // CHUNKS[kind]
        span = pl.ds(n * each, each)
        return [
            pltpu.make_async_copy(
                weight_ref.at[span, y0, y1, kind],
                held.at[kind, span, y1, y0],
                sems.at[kind, n, 2 * y1 + y0],
            )
            for y1 in range(2)
            for y0 in range(2)
        ]

    order = [(kind, n) for kind in range(kinds) for n in range(CHUNKS[kind])]

    def start(at):
        for place in order[at : at + 1]:
            for copy in copies(*place):
                copy.start()

    def arrived(kind, n):
        each = z // CHUNKS[kind]
        for copy in copies(kind, n):
            copy.wait()
        start(order.index((kind, n)) + AHEAD)
        depth = each * 4 * lines
        return held[kind, n * each : (n + 1) * each].reshape(depth, hidden_width), depth

    fetch = pltpu.make_async_copy(rows_ref, rows, rows_sem)
    fetch.start()
    for at in range(AHEAD):
        start(at)
    fetch.wait()
    sums = []
    for kind in (0, 1):
        total = None
        for n in range(CHUNKS[kind]):
            block, depth = arrived(kind, n)
            part = dot(rows[:, n * depth : (n + 1) * depth], block)
            total = part if total is None else total + part
        sums.append(total)
    gate_sum, up_sum = sums
    hidden = (gate_sum * jax.nn.sigmoid(gate_sum) * up_sum).astype(BF16)
    for n in range(CHUNKS[2]):
        block, depth = arrived(2, n)
        out_ref[:, n * depth : (n + 1) * depth] = dot_nt(hidden, block).astype(BF16)


def feed_forward(rows, weights):
    count, width = rows.shape
    z, y0, y1, kinds, lines, hidden_width = weights.shape
    return pl.pallas_call(
        ffn_kernel,
        out_shape=jax.ShapeDtypeStruct((count, width), BF16),
        in_specs=[pl.BlockSpec(memory_space=pltpu.HBM)] * 2,
        out_specs=pl.BlockSpec(memory_space=pltpu.VMEM),
        scratch_shapes=[
            pltpu.VMEM((count, width), BF16),
            pltpu.VMEM((kinds, z, y1, y0, lines, hidden_width), BF16),
            pltpu.SemaphoreType.DMA,
            pltpu.SemaphoreType.DMA((kinds, max(CHUNKS), 4)),
        ],
        cost_estimate=kernel_cost(6 * count * width * hidden_width, 2**23, count * hidden_width),
        compiler_params=pltpu.CompilerParams(vmem_limit_bytes=52 * 2**20),
        name="feed_forward",
    )(rows, weights)


def moved(value, axes, place):
    lengths = [SIZES[a] for a in axes]
    pairs = []
    for y1 in range(lengths[0]):
        for y0 in range(lengths[1]):
            for c in range(lengths[2]):
                a, b, d = place(y1, y0, c)
                pairs.append(((y1 * 2 + y0) * 2 + c, (a * 2 + b) * 2 + d))
    return lax.ppermute(value, axes, pairs)


def shifted(value, axis, by):
    length = SIZES[axis]
    return lax.ppermute(value, axis, [(i, (i + by) % length) for i in range(length)])


def exchange(tiles, axes):
    return lax.all_to_all(tiles, axes, split_axis=0, concat_axis=0, tiled=True)


def gathered_weights(gate_weight, up_weight, down_weight):
    mine = jnp.concatenate([gate_weight, up_weight, down_weight.T], axis=0)
    lines, width = mine.shape
    axes = ("y1", "y0", "c")
    near = moved(mine, axes, lambda y1, y0, c: (y1, c, y0))
    far = moved(mine, axes, lambda y1, y0, c: (1 - y1, c, y0))
    upper = lax.axis_index("y1") == 1
    pair = jnp.stack([jnp.where(upper, far, near), jnp.where(upper, near, far)])
    whole = lax.all_gather(pair, Z + ("c",), axis=0)
    return whole.reshape(16, 2, 2, 3, lines // 3, width)


def layer(
    stream,
    queries,
    keys_in,
    values_in,
    gate_in,
    log_decay,
    head_gain,
    out_weight,
    norm_gain,
    gate_weight,
    up_weight,
    down_weight,
):
    weights = gathered_weights(gate_weight, up_weight, down_weight)
    rows, width = queries.shape[0], stream.shape[1]
    head_dim = queries.shape[1]
    found = [out_weight] + [shifted(out_weight, "x", r) for r in (1, 2, 3)]
    others = [shifted(stream, "x", r) for r in (1, 2, 3)]
    near_s = jnp.stack([stream, *others])
    far_s = shifted(near_s, "y0", 1)
    near_w = jnp.concatenate(found, axis=0)
    far_w = shifted(near_w, "c", 1)
    within, carry_q, state = retention(
        queries, keys_in, values_in, log_decay.reshape(1, rows)
    )
    states = exchange(state, NEAR)
    joined = joined_state(states)
    joined = exchange(joined, "zh")
    zh = lax.axis_index("zh").astype(jnp.int32).reshape(1)
    entering = incoming_state(zh, joined, states)
    entering = exchange(entering, NEAR)
    entering = entering.reshape(head_dim, head_dim)
    sent = mix(within, carry_q, entering, gate_in, head_gain.reshape(1, -1))
    mixed = exchange(sent.reshape(16, *sent.shape[2:]), GROUP + ("c",))
    here = jnp.stack([lax.axis_index(a).astype(jnp.int32) for a in ("x", "c", "y0")])
    normed, residual = group_rows(
        here, mixed.reshape(2, 8, *mixed.shape[1:]), near_w, far_w, near_s, far_s, norm_gain.reshape(1, -1)
    )
    down_terms = feed_forward(normed, weights)
    mixer_out = exchange(down_terms.reshape(8, rows // 8, width), GROUP).astype(F32).sum(axis=0)
    return (residual + mixer_out).astype(BF16)


def solution(mesh):
    finer = Mesh(mesh.devices.reshape(*SIZES.values()), tuple(SIZES))
    return jax.shard_map(
        layer,
        mesh=finer,
        in_specs=(
            P(SP + TP, None),
            P(SP, TP),
            P(SP, TP),
            P(SP, TP),
            P(SP, TP),
            P(SP, TP),
            P(TP),
            P(TP, None),
            P(),
            P(SP, TP),
            P(SP, TP),
            P(TP, SP),
        ),
        out_specs=P(SP + TP, None),
        check_vma=False,
    )
```

profile of v0, /device:TPU:1, one launch (start us, length us, event | category | flops | bytes accessed | tf_op | source)
XLA Modules:
  0.0 167.8 jit_solution(15472120535015888683)
XLA Ops:
  6.5 0.9 pad_maximum_fusion.2
  7.5 6.0 %collective-permute-start.8 = (bf16[96,704]{1,0:T(8,128)(2,1)S(1)}, bf16[96,704]{1,0:T(8,128)(2,1)S(1)}, u32[]{:S(2)}, u32[]{:S(2)}) collective-permute-start(bf16[96,704]{1,0:T(8,128)(2,1)S(1)} %pad_maximum_fusion.2), channel_id=1, source_target_pairs={{0,16},{1,24},{8,17},{9,25},{16,0},{17,8},{24,1},{25,9},{2,18},{3,... | collective-permute-start | bytes 405512 | tf_op jit(solution)/shard_map/ppermute | solution.py:329
  13.5 1.9 %collective-permute-start.9 = (bf16[96,704]{1,0:T(8,128)(2,1)S(1)}, bf16[96,704]{1,0:T(8,128)(2,1)S(1)}, u32[]{:S(2)}, u32[]{:S(2)}) collective-permute-start(bf16[96,704]{1,0:T(8,128)(2,1)S(1)} %pad_maximum_fusion.2), channel_id=1, source_target_pairs={{0,0},{1,8},{8,1},{9,9},{16,16},{17,24},{24,17},{25,25},{2,2},{3,1... | collective-permute-start | bytes 405512 | tf_op jit(solution)/shard_map/ppermute | solution.py:329
  15.4 1.4 collective-permute-done.8
  16.9 3.1 %collective-permute-done.9 = bf16[96,704]{1,0:T(8,128)(2,1)S(1)} collective-permute-done((bf16[96,704]{1,0:T(8,128)(2,1)S(1)}, bf16[96,704]{1,0:T(8,128)(2,1)S(1)}, u32[]{:S(2)}, u32[]{:S(2)}) %collective-permute-start.9) | collective-permute-done | bytes 135200 | tf_op jit(solution)/shard_map/ppermute | solution.py:329
  20.0 0.8 pad_maximum_fusion.1
  20.8 3.3 %collective-permute-start = (bf16[128,2048]{1,0:T(8,128)(2,1)}, bf16[128,2048]{1,0:T(8,128)(2,1)S(1)}, u32[]{:S(2)}, u32[]{:S(2)}) collective-permute-start(bf16[128,2048]{1,0:T(8,128)(2,1)} %param.19), channel_id=1, source_target_pairs={{0,2},{2,4},{4,6},{6,0},{1,3},{3,5},{5,7},{7,1},{8,10},{10,12},{12... | collective-permute-start | bytes 1572872 | tf_op jit(solution)/shard_map/ppermute | solution.py:334
  24.0 4.4 %collective-permute-start.1 = (bf16[128,2048]{1,0:T(8,128)(2,1)}, bf16[128,2048]{1,0:T(8,128)(2,1)S(1)}, u32[]{:S(2)}, u32[]{:S(2)}) collective-permute-start(bf16[128,2048]{1,0:T(8,128)(2,1)} %param.19), channel_id=1, source_target_pairs={{0,4},{2,6},{4,0},{6,2},{1,5},{3,7},{5,1},{7,3},{8,12},{10,14},{12... | collective-permute-start | bytes 1572872 | tf_op jit(solution)/shard_map/ppermute | solution.py:334
  28.4 3.1 %collective-permute-start.2 = (bf16[128,2048]{1,0:T(8,128)(2,1)}, bf16[128,2048]{1,0:T(8,128)(2,1)S(1)}, u32[]{:S(2)}, u32[]{:S(2)}) collective-permute-start(bf16[128,2048]{1,0:T(8,128)(2,1)} %param.19), channel_id=1, source_target_pairs={{0,6},{2,0},{4,2},{6,4},{1,7},{3,1},{5,3},{7,5},{8,14},{10,8},{12,... | collective-permute-start | bytes 1572872 | tf_op jit(solution)/shard_map/ppermute | solution.py:334
  31.5 3.3 %collective-permute-done = bf16[128,2048]{1,0:T(8,128)(2,1)S(1)} collective-permute-done((bf16[128,2048]{1,0:T(8,128)(2,1)}, bf16[128,2048]{1,0:T(8,128)(2,1)S(1)}, u32[]{:S(2)}, u32[]{:S(2)}) %collective-permute-start) | collective-permute-done | bytes 524320 | tf_op jit(solution)/shard_map/ppermute | solution.py:334
  34.9 13.5 %collective-permute-done.1 = bf16[128,2048]{1,0:T(8,128)(2,1)S(1)} collective-permute-done((bf16[128,2048]{1,0:T(8,128)(2,1)}, bf16[128,2048]{1,0:T(8,128)(2,1)S(1)}, u32[]{:S(2)}, u32[]{:S(2)}) %collective-permute-start.1) | collective-permute-done | bytes 524320 | tf_op jit(solution)/shard_map/ppermute | solution.py:334
  48.4 2.5 %collective-permute-done.2 = bf16[128,2048]{1,0:T(8,128)(2,1)S(1)} collective-permute-done((bf16[128,2048]{1,0:T(8,128)(2,1)}, bf16[128,2048]{1,0:T(8,128)(2,1)S(1)}, u32[]{:S(2)}, u32[]{:S(2)}) %collective-permute-start.2) | collective-permute-done | bytes 524320 | tf_op jit(solution)/shard_map/ppermute | solution.py:334
  50.9 3.4 %collective-permute-start.3 = (bf16[512,2048]{1,0:T(8,128)(2,1)S(1)}, bf16[512,2048]{1,0:T(8,128)(2,1)}, u32[]{:S(2)}, u32[]{:S(2)}) collective-permute-start(bf16[512,2048]{1,0:T(8,128)(2,1)S(1)} %constant_dynamic-update-slice_fusion.near_w_ref), channel_id=1, source_target_pairs={{0,1},{1,0},{2,3},{3,2},{4,5},{5,4},{6,7},{7,6},{8,9},{9,8},{10,11... | collective-permute-start | bytes 6291464 | tf_op jit(solution)/shard_map/ppermute | solution.py:334
  54.3 1.9 %retention.1 = (f32[256,128]{1,0:T(8,128)}, bf16[256,128]{1,0:T(8,128)(2,1)}, bf16[16,16,128]{2,1,0:T(8,128)(2,1)}) custom-call(bf16[256,128]{1,0:T(8,128)(2,1)} %q_ref.1, bf16[256,128]{1,0:T(8,128)(2,1)} %k_ref.1, bf16[256,128]{1,0:T(8,128)(2,1)} %v_ref.1, f32[1,256]{1,0:T(1,128)} %bitcast.30), custom_call_target="tpu_custom_call" | custom-call | flops 50331648 | bytes 1048576 | tf_op jit(solution)/shard_map/retention/pallas_call | solution.py:83
  56.2 5.9 %all-to-all-start = ((bf16[16,16,128]{2,1,0:T(8,128)(2,1)}), bf16[16,16,128]{2,1,0:T(8,128)(2,1)S(1)}, u32[]{:S(2)}, u32[]{:S(2)}) async-start(bf16[16,16,128]{2,1,0:T(8,128)(2,1)} %get-tuple-element.12), calls=%async_computation | async-start | bytes 131072 | tf_op jit(solution)/shard_map/all_to_all | solution.py:338
  62.1 4.3 %collective-permute-start.6 = (bf16[32,2048]{1,0:T(8,128)(2,1)S(1)}, bf16[32,2048]{1,0:T(8,128)(2,1)S(1)}, u32[]{:S(2)}, u32[]{:S(2)}) collective-permute-start(bf16[32,2048]{1,0:T(8,128)(2,1)S(1)} %copy-done.3), channel_id=1, source_target_pairs={{0,6},{2,0},{4,2},{6,4},{1,7},{3,1},{5,3},{7,5},{8,14},{10,8},{12,... | collective-permute-start | bytes 393224 | tf_op jit(solution)/shard_map/ppermute | solution.py:334
  66.4 3.4 %collective-permute-start.5 = (bf16[32,2048]{1,0:T(8,128)(2,1)S(1)}, bf16[32,2048]{1,0:T(8,128)(2,1)S(1)}, u32[]{:S(2)}, u32[]{:S(2)}) collective-permute-start(bf16[32,2048]{1,0:T(8,128)(2,1)S(1)} %copy-done.3), channel_id=1, source_target_pairs={{0,4},{2,6},{4,0},{6,2},{1,5},{3,7},{5,1},{7,3},{8,12},{10,14},{12... | collective-permute-start | bytes 393224 | tf_op jit(solution)/shard_map/ppermute | solution.py:334
  69.9 1.9 %collective-permute-start.4 = (bf16[32,2048]{1,0:T(8,128)(2,1)S(1)}, bf16[32,2048]{1,0:T(8,128)(2,1)S(1)}, u32[]{:S(2)}, u32[]{:S(2)}) collective-permute-start(bf16[32,2048]{1,0:T(8,128)(2,1)S(1)} %copy-done.3), channel_id=1, source_target_pairs={{0,2},{2,4},{4,6},{6,0},{1,3},{3,5},{5,7},{7,1},{8,10},{10,12},{12... | collective-permute-start | bytes 393224 | tf_op jit(solution)/shard_map/ppermute | solution.py:334
  72.4 12.1 %all-to-all-start.1 = ((bf16[4,16,128]{2,1,0:T(8,128)(2,1)}), bf16[4,16,128]{2,1,0:T(8,128)(2,1)S(1)}, u32[]{:S(2)}, u32[]{:S(2)}) async-start(bf16[4,16,128]{2,1,0:T(8,128)(2,1)} %joined_state.1), calls=%async_computation.1 | async-start | bytes 32768 | tf_op jit(solution)/shard_map/all_to_all | solution.py:338
  84.5 11.6 %all-to-all-done.1.joined_ref = bf16[4,16,128]{2,1,0:T(8,128)(2,1)S(1)} async-done(((bf16[4,16,128]{2,1,0:T(8,128)(2,1)}), bf16[4,16,128]{2,1,0:T(8,128)(2,1)S(1)}, u32[]{:S(2)}, u32[]{:S(2)}) %all-to-all-start.1) | async-done | bytes 16416 | tf_op jit(solution)/shard_map/all_to_all | solution.py:338
  96.2 0.7 incoming_state.1
  96.8 7.1 %all-to-all-start.2 = ((bf16[16,8,128]{2,1,0:T(8,128)(2,1)}), bf16[16,8,128]{2,1,0:T(8,128)(2,1)S(1)}, u32[]{:S(2)}, u32[]{:S(2)}) async-start(bf16[16,8,128]{2,1,0:T(8,128)(2,1)} %incoming_state.1), calls=%async_computation.2 | async-start | bytes 65536 | tf_op jit(solution)/shard_map/all_to_all | solution.py:338
  104.1 3.3 %collective-permute-start.7 = (bf16[4,32,2048]{2,1,0:T(8,128)(2,1)S(1)}, bf16[4,32,2048]{2,1,0:T(8,128)(2,1)}, u32[]{:S(2)}, u32[]{:S(2)}) collective-permute-start(bf16[4,32,2048]{2,1,0:T(8,128)(2,1)S(1)} %pad_maximum_fusion.near_s_ref), channel_id=1, source_target_pairs={{0,8},{8,0},{1,9},{9,1},{2,10},{10,2},{3,11},{11,3},{4,12},{12,4},... | collective-permute-start | bytes 1572872 | tf_op jit(solution)/shard_map/ppermute | solution.py:334
  107.4 3.6 %all-to-all-done.2 = bf16[16,8,128]{2,1,0:T(8,128)(2,1)S(1)} async-done(((bf16[16,8,128]{2,1,0:T(8,128)(2,1)}), bf16[16,8,128]{2,1,0:T(8,128)(2,1)S(1)}, u32[]{:S(2)}, u32[]{:S(2)}) %all-to-all-start.2) | async-done | bytes 32800 | tf_op jit(solution)/shard_map/all_to_all | solution.py:338
  111.6 2.1 %mix.1 = bf16[8,2,4,32,128]{4,3,2,1,0:T(8,128)(2,1)} custom-call(f32[256,128]{1,0:T(8,128)} %get-tuple-element.10.within_ref, bf16[256,128]{1,0:T(8,128)(2,1)} %get-tuple-element.11.carry_q_ref, bf16[128,128]{1,0:T(8,128)(2,1)} %bitcast.24, bf16[256,128]{1,0:T(8,128)(2,1)} %gate_ref.1, bf16[1,128]{1,0:T(2,128)(2,1)} %bitcast.31), custom_call_target="tpu_custom_call" | custom-call | flops 8388608 | bytes 1048576 | tf_op jit(solution)/shard_map/mix/pallas_call | solution.py:165
  113.7 8.3 %all-to-all-start.3 = ((bf16[16,4,32,128]{3,2,1,0:T(8,128)(2,1)}), bf16[16,4,32,128]{3,2,1,0:T(8,128)(2,1)S(1)}, u32[]{:S(2)}, u32[]{:S(2)}) async-start(bf16[16,4,32,128]{3,2,1,0:T(8,128)(2,1)} %bitcast.23), calls=%async_computation.3 | async-start | bytes 1048576 | tf_op jit(solution)/shard_map/all_to_all | solution.py:338
  122.1 9.4 %all-to-all-done.3 = bf16[16,4,32,128]{3,2,1,0:T(8,128)(2,1)S(1)} async-done(((bf16[16,4,32,128]{3,2,1,0:T(8,128)(2,1)}), bf16[16,4,32,128]{3,2,1,0:T(8,128)(2,1)S(1)}, u32[]{:S(2)}, u32[]{:S(2)}) %all-to-all-start.3) | async-done | bytes 524320 | tf_op jit(solution)/shard_map/all_to_all | solution.py:338
  131.5 3.4 %group_rows.1 = (bf16[256,2048]{1,0:T(8,128)(2,1)S(1)}, f32[32,2048]{1,0:T(8,128)S(1)}) custom-call(s32[3]{0:T(128)S(1)} %pad_add_fusion.here_ref, bf16[2,8,4,32,128]{4,3,2,1,0:T(8,128)(2,1)S(1)} %bitcast.21, bf16[512,2048]{1,0:T(8,128)(2,1)S(1)} %constant_dynamic-update-slice_fusion.near_w_ref, bf16[512,2048]{1,0:T(8,128)(2,1)} %collective-permute-done.3.far_w_ref, ...), custom_call_target="tpu_custom_call" | custom-call | flops 1073741824 | bytes 8388608 | tf_op jit(solution)/shard_map/group_rows/pallas_call | solution.py:227
  134.9 1.0 copy-done
  135.9 6.4 %feed_forward.1 = bf16[256,2048]{1,0:T(8,128)(2,1)S(1)} custom-call(bf16[256,2048]{1,0:T(8,128)(2,1)} %copy-done, bf16[16,2,2,3,32,704]{5,4,3,2,1,0:T(8,128)(2,1)} %bitcast.22), custom_call_target="tpu_custom_call" | custom-call | flops 2214592512 | bytes 8388608 | tf_op jit(solution)/shard_map/feed_forward/pallas_call | solution.py:304
  142.3 17.8 %all_to_all.25 = bf16[8,32,2048]{2,1,0:T(8,128)(2,1)S(1)} all-to-all(bf16[8,32,2048]{2,1,0:T(8,128)(2,1)S(1)} %bitcast.20), channel_id=1, replica_groups=mesh['zh'=4,'zl'=4,'y1'=2,'y0'=2,'x'=4,'c'=2] {'y0','x'}, dimensions={0} | all-to-all | bytes 2097152 | tf_op jit(solution)/shard_map/all_to_all | solution.py:338
  160.3 0.7 add_convert_fusion
  (28 shorter events, 1.8 us)
Async XLA Ops:
  6.5 24.9 %copy-start.1 = (bf16[128,2048]{1,0:T(8,128)(2,1)S(1)}, bf16[128,2048]{1,0:T(8,128)(2,1)}, u32[]{:S(2)}) copy-start(bf16[128,2048]{1,0:T(8,128)(2,1)} %param.19) | copy-start | bytes 1572868
  6.5 129.4 %all-gather.3.cloned.1.call-start = ((), (), s32[]{:S(2)}) async-start(), calls=%async_computation.5 | async-start | bytes 9732096 | tf_op jit(solution)/shard_map/all_gather | solution.py:349
  7.5 9.4 %collective-permute-start.8 = (bf16[96,704]{1,0:T(8,128)(2,1)S(1)}, bf16[96,704]{1,0:T(8,128)(2,1)S(1)}, u32[]{:S(2)}, u32[]{:S(2)}) collective-permute-start(bf16[96,704]{1,0:T(8,128)(2,1)S(1)} %pad_maximum_fusion.2), channel_id=1, source_target_pairs={{0,16},{1,24},{8,17},{9,25},{16,0},{17,8},{24,1},{25,9},{2,18},{3,... | collective-permute-start | bytes 405512 | tf_op jit(solution)/shard_map/ppermute | solution.py:329
  13.5 6.5 %collective-permute-start.9 = (bf16[96,704]{1,0:T(8,128)(2,1)S(1)}, bf16[96,704]{1,0:T(8,128)(2,1)S(1)}, u32[]{:S(2)}, u32[]{:S(2)}) collective-permute-start(bf16[96,704]{1,0:T(8,128)(2,1)S(1)} %pad_maximum_fusion.2), channel_id=1, source_target_pairs={{0,0},{1,8},{8,1},{9,9},{16,16},{17,24},{24,17},{25,25},{2,2},{3,1... | collective-permute-start | bytes 405512 | tf_op jit(solution)/shard_map/ppermute | solution.py:329
  20.8 41.4 %copy-start.3 = (bf16[32,2048]{1,0:T(8,128)(2,1)S(1)}, bf16[32,2048]{1,0:T(8,128)(2,1)}, u32[]{:S(2)}) copy-start(bf16[32,2048]{1,0:T(8,128)(2,1)} %param.12) | copy-start | bytes 393220
  20.8 14.0 %collective-permute-start = (bf16[128,2048]{1,0:T(8,128)(2,1)}, bf16[128,2048]{1,0:T(8,128)(2,1)S(1)}, u32[]{:S(2)}, u32[]{:S(2)}) collective-permute-start(bf16[128,2048]{1,0:T(8,128)(2,1)} %param.19), channel_id=1, source_target_pairs={{0,2},{2,4},{4,6},{6,0},{1,3},{3,5},{5,7},{7,1},{8,10},{10,12},{12... | collective-permute-start | bytes 1572872 | tf_op jit(solution)/shard_map/ppermute | solution.py:334
  24.0 24.3 %collective-permute-start.1 = (bf16[128,2048]{1,0:T(8,128)(2,1)}, bf16[128,2048]{1,0:T(8,128)(2,1)S(1)}, u32[]{:S(2)}, u32[]{:S(2)}) collective-permute-start(bf16[128,2048]{1,0:T(8,128)(2,1)} %param.19), channel_id=1, source_target_pairs={{0,4},{2,6},{4,0},{6,2},{1,5},{3,7},{5,1},{7,3},{8,12},{10,14},{12... | collective-permute-start | bytes 1572872 | tf_op jit(solution)/shard_map/ppermute | solution.py:334
  28.4 22.5 %collective-permute-start.2 = (bf16[128,2048]{1,0:T(8,128)(2,1)}, bf16[128,2048]{1,0:T(8,128)(2,1)S(1)}, u32[]{:S(2)}, u32[]{:S(2)}) collective-permute-start(bf16[128,2048]{1,0:T(8,128)(2,1)} %param.19), channel_id=1, source_target_pairs={{0,6},{2,0},{4,2},{6,4},{1,7},{3,1},{5,3},{7,5},{8,14},{10,8},{12,... | collective-permute-start | bytes 1572872 | tf_op jit(solution)/shard_map/ppermute | solution.py:334
  48.3 73.7 %copy-start.4 = (bf16[2048]{0:T(1024)(128)(2,1)S(1)}, bf16[2048]{0:T(1024)(128)(2,1)}, u32[]{:S(2)}) copy-start(bf16[2048]{0:T(1024)(128)(2,1)} %param.20) | copy-start | bytes 12292
  50.9 80.6 %collective-permute-start.3 = (bf16[512,2048]{1,0:T(8,128)(2,1)S(1)}, bf16[512,2048]{1,0:T(8,128)(2,1)}, u32[]{:S(2)}, u32[]{:S(2)}) collective-permute-start(bf16[512,2048]{1,0:T(8,128)(2,1)S(1)} %constant_dynamic-update-slice_fusion.near_w_ref), channel_id=1, source_target_pairs={{0,1},{1,0},{2,3},{3,2},{4,5},{5,4},{6,7},{7,6},{8,9},{9,8},{10,11... | collective-permute-start | bytes 6291464 | tf_op jit(solution)/shard_map/ppermute | solution.py:334
  56.2 15.6 %all-to-all-start = ((bf16[16,16,128]{2,1,0:T(8,128)(2,1)}), bf16[16,16,128]{2,1,0:T(8,128)(2,1)S(1)}, u32[]{:S(2)}, u32[]{:S(2)}) async-start(bf16[16,16,128]{2,1,0:T(8,128)(2,1)} %get-tuple-element.12), calls=%async_computation | async-start | bytes 131072 | tf_op jit(solution)/shard_map/all_to_all | solution.py:338
  62.1 41.9 %collective-permute-start.6 = (bf16[32,2048]{1,0:T(8,128)(2,1)S(1)}, bf16[32,2048]{1,0:T(8,128)(2,1)S(1)}, u32[]{:S(2)}, u32[]{:S(2)}) collective-permute-start(bf16[32,2048]{1,0:T(8,128)(2,1)S(1)} %copy-done.3), channel_id=1, source_target_pairs={{0,6},{2,0},{4,2},{6,4},{1,7},{3,1},{5,3},{7,5},{8,14},{10,8},{12,... | collective-permute-start | bytes 393224 | tf_op jit(solution)/shard_map/ppermute | solution.py:334
  66.4 37.6 %collective-permute-start.5 = (bf16[32,2048]{1,0:T(8,128)(2,1)S(1)}, bf16[32,2048]{1,0:T(8,128)(2,1)S(1)}, u32[]{:S(2)}, u32[]{:S(2)}) collective-permute-start(bf16[32,2048]{1,0:T(8,128)(2,1)S(1)} %copy-done.3), channel_id=1, source_target_pairs={{0,4},{2,6},{4,0},{6,2},{1,5},{3,7},{5,1},{7,3},{8,12},{10,14},{12... | collective-permute-start | bytes 393224 | tf_op jit(solution)/shard_map/ppermute | solution.py:334
  69.9 34.2 %collective-permute-start.4 = (bf16[32,2048]{1,0:T(8,128)(2,1)S(1)}, bf16[32,2048]{1,0:T(8,128)(2,1)S(1)}, u32[]{:S(2)}, u32[]{:S(2)}) collective-permute-start(bf16[32,2048]{1,0:T(8,128)(2,1)S(1)} %copy-done.3), channel_id=1, source_target_pairs={{0,2},{2,4},{4,6},{6,0},{1,3},{3,5},{5,7},{7,1},{8,10},{10,12},{12... | collective-permute-start | bytes 393224 | tf_op jit(solution)/shard_map/ppermute | solution.py:334
  72.4 23.7 %all-to-all-start.1 = ((bf16[4,16,128]{2,1,0:T(8,128)(2,1)}), bf16[4,16,128]{2,1,0:T(8,128)(2,1)S(1)}, u32[]{:S(2)}, u32[]{:S(2)}) async-start(bf16[4,16,128]{2,1,0:T(8,128)(2,1)} %joined_state.1), calls=%async_computation.1 | async-start | bytes 32768 | tf_op jit(solution)/shard_map/all_to_all | solution.py:338
  96.8 14.1 %all-to-all-start.2 = ((bf16[16,8,128]{2,1,0:T(8,128)(2,1)}), bf16[16,8,128]{2,1,0:T(8,128)(2,1)S(1)}, u32[]{:S(2)}, u32[]{:S(2)}) async-start(bf16[16,8,128]{2,1,0:T(8,128)(2,1)} %incoming_state.1), calls=%async_computation.2 | async-start | bytes 65536 | tf_op jit(solution)/shard_map/all_to_all | solution.py:338
  104.1 18.0 %collective-permute-start.7 = (bf16[4,32,2048]{2,1,0:T(8,128)(2,1)S(1)}, bf16[4,32,2048]{2,1,0:T(8,128)(2,1)}, u32[]{:S(2)}, u32[]{:S(2)}) collective-permute-start(bf16[4,32,2048]{2,1,0:T(8,128)(2,1)S(1)} %pad_maximum_fusion.near_s_ref), channel_id=1, source_target_pairs={{0,8},{8,0},{1,9},{9,1},{2,10},{10,2},{3,11},{11,3},{4,12},{12,4},... | collective-permute-start | bytes 1572872 | tf_op jit(solution)/shard_map/ppermute | solution.py:334
  111.0 0.6 copy-start.2
  113.7 17.8 %all-to-all-start.3 = ((bf16[16,4,32,128]{3,2,1,0:T(8,128)(2,1)}), bf16[16,4,32,128]{3,2,1,0:T(8,128)(2,1)S(1)}, u32[]{:S(2)}, u32[]{:S(2)}) async-start(bf16[16,4,32,128]{3,2,1,0:T(8,128)(2,1)} %bitcast.23), calls=%async_computation.3 | async-start | bytes 1048576 | tf_op jit(solution)/shard_map/all_to_all | solution.py:338
  134.9 1.0 copy-start
Sparse Core Ops, SparseCore 0:
  20.9 82.8 all-gather.2
where the time goes:
time: 169 us; the launch traced here: 168 us
  starting transfers between devices  68.3 us (40%)
  waiting for transfers between devices  48.4 us (29%)
  blocking collectives  17.8 us (11%)
  Pallas kernels  15.1 us (9%)
  between operations  13.6 us (8%)
  other arithmetic  2.67 us (2%)
  local copies, waits for them, and re-layouts  1.77 us (1%)
    all_to_all x4, starting transfers between devices, exchange(): return lax.all_to_all(tiles, axes, split_axis=0, concat_axis=0, tiled=True)  33.5 us
    ppermute x8, starting transfers between devices, shifted(): lax.ppermute(value, axis, [(i, (i + by) % length) for i in range(length)])  26.9 us
    all_to_all x4, waiting for transfers between devices, exchange(): return lax.all_to_all(tiles, axes, split_axis=0, concat_axis=0, tiled=True)  24.6 us
    ppermute x8, waiting for transfers between devices, shifted(): lax.ppermute(value, axis, [(i, (i + by) % length) for i in range(length)])  19.3 us
    all_to_all x1, blocking collectives, exchange(): return lax.all_to_all(tiles, axes, split_axis=0, concat_axis=0, tiled=True)  17.8 us
    ppermute x2, starting transfers between devices, moved(): return lax.ppermute(value, axes, pairs)  7.94 us
    pallas_call x1, Pallas kernels, feed_forward(): pl.pallas_call(ffn_kernel, out_shape=jax.ShapeDtypeStruct((count, width),...  6.41 us
    ppermute x2, waiting for transfers between devices, moved(): return lax.ppermute(value, axes, pairs)  4.53 us
  transfers between devices with their start and end apart: 15, of which 8 were waited for; matrix products, arithmetic and copies ran while one was open for 0% of the time, Pallas kernels for 5%

commit v1 on v0

--- a/solution.py
+++ b/solution.py
@@ -279,8 +279,9 @@
         return held[kind, n * each : (n + 1) * each].reshape(depth, hidden_width), depth
 
     fetch = pltpu.make_async_copy(rows_ref, rows, rows_sem)
+    start(0)
     fetch.start()
-    for at in range(AHEAD):
+    for at in range(1, AHEAD):
         start(at)
     fetch.wait()
     sums = []
@@ -390,8 +391,11 @@
         here, mixed.reshape(2, 8, *mixed.shape[1:]), near_w, far_w, near_s, far_s, norm_gain.reshape(1, -1)
     )
     down_terms = feed_forward(normed, weights)
-    mixer_out = exchange(down_terms.reshape(8, rows // 8, width), GROUP).astype(F32).sum(axis=0)
-    return (residual + mixer_out).astype(BF16)
+    terms = exchange(down_terms.reshape(8, rows // 8, width), GROUP)
+    result = residual
+    for n in range(8):
+        result = result + terms[n].astype(F32)
+    return result.astype(BF16)
 
 
 def solution(mesh):

time: 169 us -> 169 us (level)
  no operation moved by 1% of the time
where the time goes in v1:
time: 169 us; the launch traced here: 168 us
  starting transfers between devices  68.3 us (40%)
  waiting for transfers between devices  48.4 us (29%)
  blocking collectives  17.8 us (11%)
  Pallas kernels  15.2 us (9%)
  between operations  13.6 us (8%)
  other arithmetic  2.65 us (2%)
  local copies, waits for them, and re-layouts  1.77 us (1%)
    all_to_all x4, starting transfers between devices, exchange(): return lax.all_to_all(tiles, axes, split_axis=0, concat_axis=0, tiled=True)  33.4 us
    ppermute x8, starting transfers between devices, shifted(): lax.ppermute(value, axis, [(i, (i + by) % length) for i in range(length)])  26.9 us
    all_to_all x4, waiting for transfers between devices, exchange(): return lax.all_to_all(tiles, axes, split_axis=0, concat_axis=0, tiled=True)  24.6 us
    ppermute x8, waiting for transfers between devices, shifted(): lax.ppermute(value, axis, [(i, (i + by) % length) for i in range(length)])  19.3 us
    all_to_all x1, blocking collectives, exchange(): return lax.all_to_all(tiles, axes, split_axis=0, concat_axis=0, tiled=True)  17.8 us
    ppermute x2, starting transfers between devices, moved(): return lax.ppermute(value, axes, pairs)  7.94 us
    pallas_call x1, Pallas kernels, feed_forward(): pl.pallas_call(ffn_kernel, out_shape=jax.ShapeDtypeStruct((count, width),...  6.41 us
    ppermute x2, waiting for transfers between devices, moved(): return lax.ppermute(value, axes, pairs)  4.53 us
  transfers between devices with their start and end apart: 15, of which 8 were waited for; matrix products, arithmetic and copies ran while one was open for 0% of the time, Pallas kernels for 5%

profile of v1, /device:TPU:1, one launch (start us, length us, event | category | flops | bytes accessed | tf_op | source)
XLA Modules:
  0.0 167.8 jit_solution(10543401639592810149)
XLA Ops:
  6.5 0.9 pad_maximum_fusion.2
  7.5 6.0 %collective-permute-start.8 = (bf16[96,704]{1,0:T(8,128)(2,1)S(1)}, bf16[96,704]{1,0:T(8,128)(2,1)S(1)}, u32[]{:S(2)}, u32[]{:S(2)}) collective-permute-start(bf16[96,704]{1,0:T(8,128)(2,1)S(1)} %pad_maximum_fusion.2), channel_id=1, source_target_pairs={{0,16},{1,24},{8,17},{9,25},{16,0},{17,8},{24,1},{25,9},{2,18},{3,... | collective-permute-start | bytes 405512 | tf_op jit(solution)/shard_map/ppermute | solution.py:330
  13.5 1.9 %collective-permute-start.9 = (bf16[96,704]{1,0:T(8,128)(2,1)S(1)}, bf16[96,704]{1,0:T(8,128)(2,1)S(1)}, u32[]{:S(2)}, u32[]{:S(2)}) collective-permute-start(bf16[96,704]{1,0:T(8,128)(2,1)S(1)} %pad_maximum_fusion.2), channel_id=1, source_target_pairs={{0,0},{1,8},{8,1},{9,9},{16,16},{17,24},{24,17},{25,25},{2,2},{3,1... | collective-permute-start | bytes 405512 | tf_op jit(solution)/shard_map/ppermute | solution.py:330
  15.4 1.4 collective-permute-done.8
  16.9 3.1 %collective-permute-done.9 = bf16[96,704]{1,0:T(8,128)(2,1)S(1)} collective-permute-done((bf16[96,704]{1,0:T(8,128)(2,1)S(1)}, bf16[96,704]{1,0:T(8,128)(2,1)S(1)}, u32[]{:S(2)}, u32[]{:S(2)}) %collective-permute-start.9) | collective-permute-done | bytes 135200 | tf_op jit(solution)/shard_map/ppermute | solution.py:330
  20.0 0.8 pad_maximum_fusion.1
  20.8 3.3 %collective-permute-start = (bf16[128,2048]{1,0:T(8,128)(2,1)}, bf16[128,2048]{1,0:T(8,128)(2,1)S(1)}, u32[]{:S(2)}, u32[]{:S(2)}) collective-permute-start(bf16[128,2048]{1,0:T(8,128)(2,1)} %param.19), channel_id=1, source_target_pairs={{0,2},{2,4},{4,6},{6,0},{1,3},{3,5},{5,7},{7,1},{8,10},{10,12},{12... | collective-permute-start | bytes 1572872 | tf_op jit(solution)/shard_map/ppermute | solution.py:335
  24.0 4.4 %collective-permute-start.1 = (bf16[128,2048]{1,0:T(8,128)(2,1)}, bf16[128,2048]{1,0:T(8,128)(2,1)S(1)}, u32[]{:S(2)}, u32[]{:S(2)}) collective-permute-start(bf16[128,2048]{1,0:T(8,128)(2,1)} %param.19), channel_id=1, source_target_pairs={{0,4},{2,6},{4,0},{6,2},{1,5},{3,7},{5,1},{7,3},{8,12},{10,14},{12... | collective-permute-start | bytes 1572872 | tf_op jit(solution)/shard_map/ppermute | solution.py:335
  28.4 3.1 %collective-permute-start.2 = (bf16[128,2048]{1,0:T(8,128)(2,1)}, bf16[128,2048]{1,0:T(8,128)(2,1)S(1)}, u32[]{:S(2)}, u32[]{:S(2)}) collective-permute-start(bf16[128,2048]{1,0:T(8,128)(2,1)} %param.19), channel_id=1, source_target_pairs={{0,6},{2,0},{4,2},{6,4},{1,7},{3,1},{5,3},{7,5},{8,14},{10,8},{12,... | collective-permute-start | bytes 1572872 | tf_op jit(solution)/shard_map/ppermute | solution.py:335
  31.5 3.3 %collective-permute-done = bf16[128,2048]{1,0:T(8,128)(2,1)S(1)} collective-permute-done((bf16[128,2048]{1,0:T(8,128)(2,1)}, bf16[128,2048]{1,0:T(8,128)(2,1)S(1)}, u32[]{:S(2)}, u32[]{:S(2)}) %collective-permute-start) | collective-permute-done | bytes 524320 | tf_op jit(solution)/shard_map/ppermute | solution.py:335
  34.8 13.5 %collective-permute-done.1 = bf16[128,2048]{1,0:T(8,128)(2,1)S(1)} collective-permute-done((bf16[128,2048]{1,0:T(8,128)(2,1)}, bf16[128,2048]{1,0:T(8,128)(2,1)S(1)}, u32[]{:S(2)}, u32[]{:S(2)}) %collective-permute-start.1) | collective-permute-done | bytes 524320 | tf_op jit(solution)/shard_map/ppermute | solution.py:335
  48.4 2.5 %collective-permute-done.2 = bf16[128,2048]{1,0:T(8,128)(2,1)S(1)} collective-permute-done((bf16[128,2048]{1,0:T(8,128)(2,1)}, bf16[128,2048]{1,0:T(8,128)(2,1)S(1)}, u32[]{:S(2)}, u32[]{:S(2)}) %collective-permute-start.2) | collective-permute-done | bytes 524320 | tf_op jit(solution)/shard_map/ppermute | solution.py:335
  50.9 3.4 %collective-permute-start.3 = (bf16[512,2048]{1,0:T(8,128)(2,1)S(1)}, bf16[512,2048]{1,0:T(8,128)(2,1)}, u32[]{:S(2)}, u32[]{:S(2)}) collective-permute-start(bf16[512,2048]{1,0:T(8,128)(2,1)S(1)} %constant_dynamic-update-slice_fusion.near_w_ref), channel_id=1, source_target_pairs={{0,1},{1,0},{2,3},{3,2},{4,5},{5,4},{6,7},{7,6},{8,9},{9,8},{10,11... | collective-permute-start | bytes 6291464 | tf_op jit(solution)/shard_map/ppermute | solution.py:335
  54.3 1.9 %retention.1 = (f32[256,128]{1,0:T(8,128)}, bf16[256,128]{1,0:T(8,128)(2,1)}, bf16[16,16,128]{2,1,0:T(8,128)(2,1)}) custom-call(bf16[256,128]{1,0:T(8,128)(2,1)} %q_ref.1, bf16[256,128]{1,0:T(8,128)(2,1)} %k_ref.1, bf16[256,128]{1,0:T(8,128)(2,1)} %v_ref.1, f32[1,256]{1,0:T(1,128)} %bitcast.70), custom_call_target="tpu_custom_call" | custom-call | flops 50331648 | bytes 1048576 | tf_op jit(solution)/shard_map/retention/pallas_call | solution.py:83
  56.2 5.9 %all-to-all-start = ((bf16[16,16,128]{2,1,0:T(8,128)(2,1)}), bf16[16,16,128]{2,1,0:T(8,128)(2,1)S(1)}, u32[]{:S(2)}, u32[]{:S(2)}) async-start(bf16[16,16,128]{2,1,0:T(8,128)(2,1)} %get-tuple-element.12), calls=%async_computation | async-start | bytes 131072 | tf_op jit(solution)/shard_map/all_to_all | solution.py:339
  62.1 4.3 %collective-permute-start.6 = (bf16[32,2048]{1,0:T(8,128)(2,1)S(1)}, bf16[32,2048]{1,0:T(8,128)(2,1)S(1)}, u32[]{:S(2)}, u32[]{:S(2)}) collective-permute-start(bf16[32,2048]{1,0:T(8,128)(2,1)S(1)} %copy-done.3), channel_id=1, source_target_pairs={{0,6},{2,0},{4,2},{6,4},{1,7},{3,1},{5,3},{7,5},{8,14},{10,8},{12,... | collective-permute-start | bytes 393224 | tf_op jit(solution)/shard_map/ppermute | solution.py:335
  66.4 3.4 %collective-permute-start.5 = (bf16[32,2048]{1,0:T(8,128)(2,1)S(1)}, bf16[32,2048]{1,0:T(8,128)(2,1)S(1)}, u32[]{:S(2)}, u32[]{:S(2)}) collective-permute-start(bf16[32,2048]{1,0:T(8,128)(2,1)S(1)} %copy-done.3), channel_id=1, source_target_pairs={{0,4},{2,6},{4,0},{6,2},{1,5},{3,7},{5,1},{7,3},{8,12},{10,14},{12... | collective-permute-start | bytes 393224 | tf_op jit(solution)/shard_map/ppermute | solution.py:335
  69.9 1.9 %collective-permute-start.4 = (bf16[32,2048]{1,0:T(8,128)(2,1)S(1)}, bf16[32,2048]{1,0:T(8,128)(2,1)S(1)}, u32[]{:S(2)}, u32[]{:S(2)}) collective-permute-start(bf16[32,2048]{1,0:T(8,128)(2,1)S(1)} %copy-done.3), channel_id=1, source_target_pairs={{0,2},{2,4},{4,6},{6,0},{1,3},{3,5},{5,7},{7,1},{8,10},{10,12},{12... | collective-permute-start | bytes 393224 | tf_op jit(solution)/shard_map/ppermute | solution.py:335
  72.5 12.1 %all-to-all-start.1 = ((bf16[4,16,128]{2,1,0:T(8,128)(2,1)}), bf16[4,16,128]{2,1,0:T(8,128)(2,1)S(1)}, u32[]{:S(2)}, u32[]{:S(2)}) async-start(bf16[4,16,128]{2,1,0:T(8,128)(2,1)} %joined_state.1), calls=%async_computation.1 | async-start | bytes 32768 | tf_op jit(solution)/shard_map/all_to_all | solution.py:339
  84.6 11.6 %all-to-all-done.1.joined_ref = bf16[4,16,128]{2,1,0:T(8,128)(2,1)S(1)} async-done(((bf16[4,16,128]{2,1,0:T(8,128)(2,1)}), bf16[4,16,128]{2,1,0:T(8,128)(2,1)S(1)}, u32[]{:S(2)}, u32[]{:S(2)}) %all-to-all-start.1) | async-done | bytes 16416 | tf_op jit(solution)/shard_map/all_to_all | solution.py:339
  96.2 0.7 incoming_state.1
  96.9 7.2 %all-to-all-start.2 = ((bf16[16,8,128]{2,1,0:T(8,128)(2,1)}), bf16[16,8,128]{2,1,0:T(8,128)(2,1)S(1)}, u32[]{:S(2)}, u32[]{:S(2)}) async-start(bf16[16,8,128]{2,1,0:T(8,128)(2,1)} %incoming_state.1), calls=%async_computation.2 | async-start | bytes 65536 | tf_op jit(solution)/shard_map/all_to_all | solution.py:339
  104.2 3.3 %collective-permute-start.7 = (bf16[4,32,2048]{2,1,0:T(8,128)(2,1)S(1)}, bf16[4,32,2048]{2,1,0:T(8,128)(2,1)}, u32[]{:S(2)}, u32[]{:S(2)}) collective-permute-start(bf16[4,32,2048]{2,1,0:T(8,128)(2,1)S(1)} %pad_maximum_fusion.near_s_ref), channel_id=1, source_target_pairs={{0,8},{8,0},{1,9},{9,1},{2,10},{10,2},{3,11},{11,3},{4,12},{12,4},... | collective-permute-start | bytes 1572872 | tf_op jit(solution)/shard_map/ppermute | solution.py:335
  107.5 3.6 %all-to-all-done.2 = bf16[16,8,128]{2,1,0:T(8,128)(2,1)S(1)} async-done(((bf16[16,8,128]{2,1,0:T(8,128)(2,1)}), bf16[16,8,128]{2,1,0:T(8,128)(2,1)S(1)}, u32[]{:S(2)}, u32[]{:S(2)}) %all-to-all-start.2) | async-done | bytes 32800 | tf_op jit(solution)/shard_map/all_to_all | solution.py:339
  111.7 2.1 %mix.1 = bf16[8,2,4,32,128]{4,3,2,1,0:T(8,128)(2,1)} custom-call(f32[256,128]{1,0:T(8,128)} %get-tuple-element.10.within_ref, bf16[256,128]{1,0:T(8,128)(2,1)} %get-tuple-element.11.carry_q_ref, bf16[128,128]{1,0:T(8,128)(2,1)} %bitcast.64, bf16[256,128]{1,0:T(8,128)(2,1)} %gate_ref.1, bf16[1,128]{1,0:T(2,128)(2,1)} %bitcast.71), custom_call_target="tpu_custom_call" | custom-call | flops 8388608 | bytes 1048576 | tf_op jit(solution)/shard_map/mix/pallas_call | solution.py:165
  113.8 8.2 %all-to-all-start.3 = ((bf16[16,4,32,128]{3,2,1,0:T(8,128)(2,1)}), bf16[16,4,32,128]{3,2,1,0:T(8,128)(2,1)S(1)}, u32[]{:S(2)}, u32[]{:S(2)}) async-start(bf16[16,4,32,128]{3,2,1,0:T(8,128)(2,1)} %bitcast.63), calls=%async_computation.3 | async-start | bytes 1048576 | tf_op jit(solution)/shard_map/all_to_all | solution.py:339
  122.1 9.4 %all-to-all-done.3 = bf16[16,4,32,128]{3,2,1,0:T(8,128)(2,1)S(1)} async-done(((bf16[16,4,32,128]{3,2,1,0:T(8,128)(2,1)}), bf16[16,4,32,128]{3,2,1,0:T(8,128)(2,1)S(1)}, u32[]{:S(2)}, u32[]{:S(2)}) %all-to-all-start.3) | async-done | bytes 524320 | tf_op jit(solution)/shard_map/all_to_all | solution.py:339
  131.5 3.4 %group_rows.1 = (bf16[256,2048]{1,0:T(8,128)(2,1)S(1)}, f32[32,2048]{1,0:T(8,128)S(1)}) custom-call(s32[3]{0:T(128)S(1)} %pad_add_fusion.here_ref, bf16[2,8,4,32,128]{4,3,2,1,0:T(8,128)(2,1)S(1)} %bitcast.61, bf16[512,2048]{1,0:T(8,128)(2,1)S(1)} %constant_dynamic-update-slice_fusion.near_w_ref, bf16[512,2048]{1,0:T(8,128)(2,1)} %collective-permute-done.3.far_w_ref, ...), custom_call_target="tpu_custom_call" | custom-call | flops 1073741824 | bytes 8388608 | tf_op jit(solution)/shard_map/group_rows/pallas_call | solution.py:227
  134.9 1.0 copy-done
  135.9 6.4 %feed_forward.1 = bf16[256,2048]{1,0:T(8,128)(2,1)S(1)} custom-call(bf16[256,2048]{1,0:T(8,128)(2,1)} %copy-done, bf16[16,2,2,3,32,704]{5,4,3,2,1,0:T(8,128)(2,1)} %bitcast.62), custom_call_target="tpu_custom_call" | custom-call | flops 2214592512 | bytes 8388608 | tf_op jit(solution)/shard_map/feed_forward/pallas_call | solution.py:305
  142.3 17.8 %all_to_all.25 = bf16[8,32,2048]{2,1,0:T(8,128)(2,1)S(1)} all-to-all(bf16[8,32,2048]{2,1,0:T(8,128)(2,1)S(1)} %bitcast.60), channel_id=1, replica_groups=mesh['zh'=4,'zl'=4,'y1'=2,'y0'=2,'x'=4,'c'=2] {'y0','x'}, dimensions={0} | all-to-all | bytes 2097152 | tf_op jit(solution)/shard_map/all_to_all | solution.py:339
  160.2 0.8 fusion
  (27 shorter events, 1.6 us)
Async XLA Ops:
  6.5 24.9 %copy-start.1 = (bf16[128,2048]{1,0:T(8,128)(2,1)S(1)}, bf16[128,2048]{1,0:T(8,128)(2,1)}, u32[]{:S(2)}) copy-start(bf16[128,2048]{1,0:T(8,128)(2,1)} %param.19) | copy-start | bytes 1572868
  6.5 129.4 %all-gather.3.cloned.1.call-start = ((), (), s32[]{:S(2)}) async-start(), calls=%async_computation.5 | async-start | bytes 9732096 | tf_op jit(solution)/shard_map/all_gather | solution.py:350
  7.5 9.4 %collective-permute-start.8 = (bf16[96,704]{1,0:T(8,128)(2,1)S(1)}, bf16[96,704]{1,0:T(8,128)(2,1)S(1)}, u32[]{:S(2)}, u32[]{:S(2)}) collective-permute-start(bf16[96,704]{1,0:T(8,128)(2,1)S(1)} %pad_maximum_fusion.2), channel_id=1, source_target_pairs={{0,16},{1,24},{8,17},{9,25},{16,0},{17,8},{24,1},{25,9},{2,18},{3,... | collective-permute-start | bytes 405512 | tf_op jit(solution)/shard_map/ppermute | solution.py:330
  13.5 6.5 %collective-permute-start.9 = (bf16[96,704]{1,0:T(8,128)(2,1)S(1)}, bf16[96,704]{1,0:T(8,128)(2,1)S(1)}, u32[]{:S(2)}, u32[]{:S(2)}) collective-permute-start(bf16[96,704]{1,0:T(8,128)(2,1)S(1)} %pad_maximum_fusion.2), channel_id=1, source_target_pairs={{0,0},{1,8},{8,1},{9,9},{16,16},{17,24},{24,17},{25,25},{2,2},{3,1... | collective-permute-start | bytes 405512 | tf_op jit(solution)/shard_map/ppermute | solution.py:330
  20.8 41.4 %copy-start.3 = (bf16[32,2048]{1,0:T(8,128)(2,1)S(1)}, bf16[32,2048]{1,0:T(8,128)(2,1)}, u32[]{:S(2)}) copy-start(bf16[32,2048]{1,0:T(8,128)(2,1)} %param.12) | copy-start | bytes 393220
  20.8 14.0 %collective-permute-start = (bf16[128,2048]{1,0:T(8,128)(2,1)}, bf16[128,2048]{1,0:T(8,128)(2,1)S(1)}, u32[]{:S(2)}, u32[]{:S(2)}) collective-permute-start(bf16[128,2048]{1,0:T(8,128)(2,1)} %param.19), channel_id=1, source_target_pairs={{0,2},{2,4},{4,6},{6,0},{1,3},{3,5},{5,7},{7,1},{8,10},{10,12},{12... | collective-permute-start | bytes 1572872 | tf_op jit(solution)/shard_map/ppermute | solution.py:335
  24.0 24.3 %collective-permute-start.1 = (bf16[128,2048]{1,0:T(8,128)(2,1)}, bf16[128,2048]{1,0:T(8,128)(2,1)S(1)}, u32[]{:S(2)}, u32[]{:S(2)}) collective-permute-start(bf16[128,2048]{1,0:T(8,128)(2,1)} %param.19), channel_id=1, source_target_pairs={{0,4},{2,6},{4,0},{6,2},{1,5},{3,7},{5,1},{7,3},{8,12},{10,14},{12... | collective-permute-start | bytes 1572872 | tf_op jit(solution)/shard_map/ppermute | solution.py:335
  28.4 22.5 %collective-permute-start.2 = (bf16[128,2048]{1,0:T(8,128)(2,1)}, bf16[128,2048]{1,0:T(8,128)(2,1)S(1)}, u32[]{:S(2)}, u32[]{:S(2)}) collective-permute-start(bf16[128,2048]{1,0:T(8,128)(2,1)} %param.19), channel_id=1, source_target_pairs={{0,6},{2,0},{4,2},{6,4},{1,7},{3,1},{5,3},{7,5},{8,14},{10,8},{12,... | collective-permute-start | bytes 1572872 | tf_op jit(solution)/shard_map/ppermute | solution.py:335
  48.3 73.7 %copy-start.4 = (bf16[2048]{0:T(1024)(128)(2,1)S(1)}, bf16[2048]{0:T(1024)(128)(2,1)}, u32[]{:S(2)}) copy-start(bf16[2048]{0:T(1024)(128)(2,1)} %param.20) | copy-start | bytes 12292
  50.9 80.6 %collective-permute-start.3 = (bf16[512,2048]{1,0:T(8,128)(2,1)S(1)}, bf16[512,2048]{1,0:T(8,128)(2,1)}, u32[]{:S(2)}, u32[]{:S(2)}) collective-permute-start(bf16[512,2048]{1,0:T(8,128)(2,1)S(1)} %constant_dynamic-update-slice_fusion.near_w_ref), channel_id=1, source_target_pairs={{0,1},{1,0},{2,3},{3,2},{4,5},{5,4},{6,7},{7,6},{8,9},{9,8},{10,11... | collective-permute-start | bytes 6291464 | tf_op jit(solution)/shard_map/ppermute | solution.py:335
  56.2 15.6 %all-to-all-start = ((bf16[16,16,128]{2,1,0:T(8,128)(2,1)}), bf16[16,16,128]{2,1,0:T(8,128)(2,1)S(1)}, u32[]{:S(2)}, u32[]{:S(2)}) async-start(bf16[16,16,128]{2,1,0:T(8,128)(2,1)} %get-tuple-element.12), calls=%async_computation | async-start | bytes 131072 | tf_op jit(solution)/shard_map/all_to_all | solution.py:339
  62.1 42.0 %collective-permute-start.6 = (bf16[32,2048]{1,0:T(8,128)(2,1)S(1)}, bf16[32,2048]{1,0:T(8,128)(2,1)S(1)}, u32[]{:S(2)}, u32[]{:S(2)}) collective-permute-start(bf16[32,2048]{1,0:T(8,128)(2,1)S(1)} %copy-done.3), channel_id=1, source_target_pairs={{0,6},{2,0},{4,2},{6,4},{1,7},{3,1},{5,3},{7,5},{8,14},{10,8},{12,... | collective-permute-start | bytes 393224 | tf_op jit(solution)/shard_map/ppermute | solution.py:335
  66.4 37.7 %collective-permute-start.5 = (bf16[32,2048]{1,0:T(8,128)(2,1)S(1)}, bf16[32,2048]{1,0:T(8,128)(2,1)S(1)}, u32[]{:S(2)}, u32[]{:S(2)}) collective-permute-start(bf16[32,2048]{1,0:T(8,128)(2,1)S(1)} %copy-done.3), channel_id=1, source_target_pairs={{0,4},{2,6},{4,0},{6,2},{1,5},{3,7},{5,1},{7,3},{8,12},{10,14},{12... | collective-permute-start | bytes 393224 | tf_op jit(solution)/shard_map/ppermute | solution.py:335
  69.9 34.3 %collective-permute-start.4 = (bf16[32,2048]{1,0:T(8,128)(2,1)S(1)}, bf16[32,2048]{1,0:T(8,128)(2,1)S(1)}, u32[]{:S(2)}, u32[]{:S(2)}) collective-permute-start(bf16[32,2048]{1,0:T(8,128)(2,1)S(1)} %copy-done.3), channel_id=1, source_target_pairs={{0,2},{2,4},{4,6},{6,0},{1,3},{3,5},{5,7},{7,1},{8,10},{10,12},{12... | collective-permute-start | bytes 393224 | tf_op jit(solution)/shard_map/ppermute | solution.py:335
  72.5 23.7 %all-to-all-start.1 = ((bf16[4,16,128]{2,1,0:T(8,128)(2,1)}), bf16[4,16,128]{2,1,0:T(8,128)(2,1)S(1)}, u32[]{:S(2)}, u32[]{:S(2)}) async-start(bf16[4,16,128]{2,1,0:T(8,128)(2,1)} %joined_state.1), calls=%async_computation.1 | async-start | bytes 32768 | tf_op jit(solution)/shard_map/all_to_all | solution.py:339
  96.9 14.2 %all-to-all-start.2 = ((bf16[16,8,128]{2,1,0:T(8,128)(2,1)}), bf16[16,8,128]{2,1,0:T(8,128)(2,1)S(1)}, u32[]{:S(2)}, u32[]{:S(2)}) async-start(bf16[16,8,128]{2,1,0:T(8,128)(2,1)} %incoming_state.1), calls=%async_computation.2 | async-start | bytes 65536 | tf_op jit(solution)/shard_map/all_to_all | solution.py:339
  104.2 17.9 %collective-permute-start.7 = (bf16[4,32,2048]{2,1,0:T(8,128)(2,1)S(1)}, bf16[4,32,2048]{2,1,0:T(8,128)(2,1)}, u32[]{:S(2)}, u32[]{:S(2)}) collective-permute-start(bf16[4,32,2048]{2,1,0:T(8,128)(2,1)S(1)} %pad_maximum_fusion.near_s_ref), channel_id=1, source_target_pairs={{0,8},{8,0},{1,9},{9,1},{2,10},{10,2},{3,11},{11,3},{4,12},{12,4},... | collective-permute-start | bytes 1572872 | tf_op jit(solution)/shard_map/ppermute | solution.py:335
  111.1 0.6 copy-start.2
  113.8 17.7 %all-to-all-start.3 = ((bf16[16,4,32,128]{3,2,1,0:T(8,128)(2,1)}), bf16[16,4,32,128]{3,2,1,0:T(8,128)(2,1)S(1)}, u32[]{:S(2)}, u32[]{:S(2)}) async-start(bf16[16,4,32,128]{3,2,1,0:T(8,128)(2,1)} %bitcast.63), calls=%async_computation.3 | async-start | bytes 1048576 | tf_op jit(solution)/shard_map/all_to_all | solution.py:339
  134.9 1.0 copy-start
Sparse Core Ops, SparseCore 0:
  20.9 82.8 all-gather.2
